TPU v7x, 32 devices: a whole 2x2x4 slice. The times are simulated.
32 devices in a mesh: sp: 8 (over z, core), tp: 4 (over y, x).
Axes of the slice: x: 2, y: 2, z: 4, core: 2. Of those that a mesh axis runs over, the one named last changes fastest.
Arguments:
- resid: bfloat16 [4096, 2048], P(('sp', 'tp')), may hold values from -6 to 6
- branch_input: bfloat16 [1024, 4096], P('tp', 'sp'), may hold values from -6 to 6
- gate_in: bfloat16 [1024, 4096], P('tp', 'sp'), may hold values from -6 to 6
- conv_taps: bfloat16 [4, 1024], P(None, 'tp'), may hold values from -3 to 3
- rate_weight: bfloat16 [16, 64, 64], P('tp'), may hold values from -0.75 to 0.75
- input_weight: bfloat16 [16, 64, 64], P('tp'), may hold values from -0.75 to 0.75
- decay_base: float32 [1024], P('tp')
- decay_extra: float32 [4096], P('sp'), may hold values from -2 to 0
- out_weight: bfloat16 [1024, 2048], P('tp'), may hold values from -0.1875 to 0.1875
- gain_mix: float32 [2048], replicated, may hold values from 0.1 to 1.9
- gain_pre: float32 [2048], replicated, may hold values from 0.1 to 1.9
- gain_post: float32 [2048], replicated, may hold values from 0.1 to 1.9
- expert_ids: int32 [4096, 2], P(('sp', 'tp')), may hold values from 0 to 7, as said below
- route_weight: float32 [4096, 2], P(('sp', 'tp')), may hold values from 0.2 to 1
- gate_proj: bfloat16 [8, 512, 2048], P('sp', 'tp'), may hold values from -0.125 to 0.125
- up_proj: bfloat16 [8, 512, 2048], P('sp', 'tp'), may hold values from -0.125 to 0.125
- down_proj: bfloat16 [8, 512, 2048], P('sp', 'tp'), may hold values from -0.25 to 0.25
Outputs:
- layer_out: bfloat16 [4096, 2048], P(('sp', 'tp'))
Inputs may be any that keep to these rules, and one draw needn't show every extreme that they name: `expert_ids`: each row names two different experts of one group: both lie in g * 2 .. g * 2 + 1 for some g. In each aligned block of 128 rows (the rows of one device) every expert is named by exactly 32 rows.
All inputs are finite; a program needn't handle non-finite values.
Results may differ from a plain program's by a relative error of at most 0.0065.
Values may be sent and summed in bfloat16 or wider, within the bound.
A program may use at most 128 MiB of HBM per device.

v0:
```python
import math
import jax
import jax.numpy as jnp
from jax import lax
from jax.sharding import PartitionSpec as P

epsilon = 1e-06
gate_power = 8.0


def entering_2(array, axis, combine, identity):
    count, here = (lax.axis_size(axis), lax.axis_index(axis))
    everything = jax.tree.map(lambda part: lax.all_gather(part, axis), array)
    start = jax.tree.map(
        lambda part, zero: jnp.broadcast_to(jnp.asarray(zero, part.dtype), part.shape),
        array,
        identity,
    )

    def hop(k, before):
        reached = k < here
        new = combine(before, jax.tree.map(lambda part: part[k], everything))
        return jax.tree.map(lambda a, b: jnp.where(reached, a, b), new, before)

    return lax.fori_loop(0, count, hop, start)


def passed_along(value, axis, steps):
    count = lax.axis_size(axis)
    first, last = (max(0, -steps), min(count, count - steps))
    return lax.ppermute(value, axis, [(source, source + steps) for source in range(first, last)])


def normalized(values, gain):
    return values * lax.rsqrt(jnp.mean(values * values, axis=-1, keepdims=True) + epsilon) * gain


def combine_pair(earlier, latter):
    return (earlier[0] * latter[0], latter[0] * earlier[1] + latter[1])


def carry_in(block_keep, block_state):
    identity = (jnp.ones(block_keep.shape, jnp.float32), jnp.zeros(block_state.shape, jnp.float32))
    return entering_2((block_keep, block_state), "sp", combine_pair, identity)


def block_cumsum(log_keep):
    channels, positions = log_keep.shape
    span = math.gcd(positions, 128)
    count = positions // span
    shaped = log_keep.reshape(channels, count, span)
    inner = jnp.cumsum(shaped, axis=2)
    before = jnp.cumsum(inner[:, :, -1], axis=1) - inner[:, :, -1]
    return (inner + before[:, :, None]).reshape(channels, positions)


def block_recurrence(log_keep, driven, start_state):
    channels, positions = log_keep.shape
    span = math.gcd(positions, 128)
    count = positions // span
    order = jnp.arange(span, dtype=jnp.int32)
    lower = (order[:, None] >= order[None, :])[None, :, :]

    def one_block(index, carried):
        state, total_log, states_out, logs_out = carried
        first = index * span
        block_log = lax.dynamic_slice_in_dim(log_keep, first, span, 1)
        block_drive = lax.dynamic_slice_in_dim(driven, first, span, 1)
        running = jnp.cumsum(block_log, axis=1)
        gap = jnp.where(lower, running[:, :, None] - running[:, None, :], -jnp.inf)
        inner = jnp.einsum("cts,cs->ct", jnp.exp(gap), block_drive, precision=lax.Precision.HIGHEST)
        produced = inner + jnp.exp(running) * state[:, None]
        whole_log = running + total_log[:, None]
        states_out = lax.dynamic_update_slice_in_dim(states_out, produced, first, 1)
        logs_out = lax.dynamic_update_slice_in_dim(logs_out, whole_log, first, 1)
        return (produced[:, -1], whole_log[:, -1], states_out, logs_out)

    initial = (
        start_state,
        jnp.zeros((channels,), jnp.float32),
        jnp.zeros((channels, positions), jnp.float32),
        jnp.zeros((channels, positions), jnp.float32),
    )
    _, _, hidden_state, summed_log = lax.fori_loop(0, count, one_block, initial)
    return (hidden_state, summed_log)


def per_device(
    resid,
    branch_input,
    gate_in,
    conv_taps,
    rate_weight,
    input_weight,
    decay_base,
    decay_extra,
    out_weight,
    gain_mix,
    gain_pre,
    gain_post,
    expert_ids,
    route_weight,
    gate_proj,
    up_proj,
    down_proj,
):
    channels, positions = branch_input.shape
    tap_count = conv_taps.shape[0]
    edge_cols = passed_along(branch_input[:, positions - (tap_count - 1) :], "sp", 1)
    padded = jnp.concatenate([edge_cols, branch_input], axis=1).astype(jnp.float32)
    filter_tap_weights = conv_taps.astype(jnp.float32)
    convolved = filter_tap_weights[0][:, None] * padded[:, 0:positions]
    for offset in range(1, tap_count):
        convolved = (
            convolved + filter_tap_weights[offset][:, None] * padded[:, offset : offset + positions]
        )
    grouped = convolved.reshape(rate_weight.shape[0], rate_weight.shape[1], positions)
    rate_gate = jax.nn.sigmoid(
        jnp.einsum(
            "ncs,ncd->nds",
            grouped,
            rate_weight.astype(jnp.float32),
            precision=lax.Precision.HIGHEST,
        ).reshape(channels, positions)
    )
    input_gate = jax.nn.sigmoid(
        jnp.einsum(
            "ncs,ncd->nds",
            grouped,
            input_weight.astype(jnp.float32),
            precision=lax.Precision.HIGHEST,
        ).reshape(channels, positions)
    )
    decay_rate = -gate_power * jax.nn.softplus(-decay_base)
    log_keep = decay_rate[:, None] * rate_gate + decay_extra[None, :]
    driven = jnp.sqrt(-jnp.expm1(2.0 * log_keep)) * input_gate * convolved
    summed_log = block_cumsum(log_keep)
    tail_keep = jnp.exp(summed_log[:, -1:] - summed_log)
    _, entering = carry_in(jnp.exp(summed_log[:, -1]), jnp.sum(driven * tail_keep, axis=1))
    hidden_state = block_recurrence(log_keep, driven, entering)[0]
    branch_out = (hidden_state * jax.nn.gelu(gate_in.astype(jnp.float32), approximate=True)).astype(
        jnp.bfloat16
    )
    token_rows = lax.all_to_all(branch_out, "tp", split_axis=1, concat_axis=0, tiled=True)
    token_count = token_rows.shape[1]
    mixed_rows = lax.dot_general(
        token_rows,
        lax.all_gather(out_weight, "tp", axis=0, tiled=True),
        (((0,), (0,)), ((), ())),
        preferred_element_type=jnp.float32,
    )
    after_mix = resid.astype(jnp.float32) + normalized(mixed_rows, gain_mix)
    ffn_in = normalized(after_mix, gain_pre).astype(jnp.bfloat16)
    top_count = expert_ids.shape[1]
    experts = gate_proj.shape[0] * lax.axis_size("sp")
    capacity = top_count * token_count // experts
    chosen = expert_ids.reshape(-1)
    matches = (chosen[:, None] == jnp.arange(experts, dtype=jnp.int32)[None, :]).astype(jnp.int32)
    slot_index = jnp.sum((jnp.cumsum(matches, axis=0) - 1) * matches, axis=1)
    target = chosen * capacity + slot_index
    source = (
        jnp.zeros((experts * capacity,), jnp.int32)
        .at[target]
        .set(jnp.arange(token_count * top_count, dtype=jnp.int32) // top_count)
    )
    outgoing = ffn_in[source].reshape(experts, capacity, ffn_in.shape[1])
    arriving = lax.all_to_all(outgoing, "sp", split_axis=0, concat_axis=1, tiled=True)
    gate_rows = lax.all_gather(gate_proj, "tp", axis=1, tiled=True)
    up_rows = lax.all_gather(up_proj, "tp", axis=1, tiled=True)
    down_rows = lax.all_gather(down_proj, "tp", axis=1, tiled=True)
    gate_vals = jnp.einsum("emd,ekd->emk", arriving, gate_rows, preferred_element_type=jnp.float32)
    up_vals = jnp.einsum("emd,ekd->emk", arriving, up_rows, preferred_element_type=jnp.float32)
    hidden = (jax.nn.silu(gate_vals) * up_vals).astype(jnp.bfloat16)
    result = jnp.einsum("emk,ekd->emd", hidden, down_rows, preferred_element_type=jnp.float32)
    returned = lax.all_to_all(
        result.astype(jnp.bfloat16), "sp", split_axis=1, concat_axis=0, tiled=True
    )
    returned = returned.reshape(experts * capacity, returned.shape[2])
    picked = returned[target].astype(jnp.float32).reshape(token_count, top_count, returned.shape[1])
    moe = jnp.sum(picked * route_weight[:, :, None], axis=1)
    return (after_mix + normalized(moe, gain_post)).astype(jnp.bfloat16)


def solution(mesh):
    in_specs = (
        P(("sp", "tp"), None),
        P("tp", "sp"),
        P("tp", "sp"),
        P(None, "tp"),
        P("tp", None, None),
        P("tp", None, None),
        P("tp"),
        P("sp"),
        P("tp", None),
        P(),
        P(),
        P(),
        P(("sp", "tp"), None),
        P(("sp", "tp"), None),
        P("sp", "tp", None),
        P("sp", "tp", None),
        P("sp", "tp", None),
    )
    out_specs = P(("sp", "tp"), None)
    return jax.shard_map(
        per_device, mesh=mesh, in_specs=in_specs, out_specs=out_specs, check_vma=False
    )
```

profile of v0, /device:TPU:0, one launch (start us, length us, event | category | flops | bytes accessed | tf_op | source)
XLA Modules:
  0.0 288.3 jit_solution(16945330147929977153)
XLA Ops:
  6.6 0.7 all-gather.8.cloned.1.call-update
  7.3 0.7 all-gather.10.cloned.1.call-update
  8.1 0.7 all-gather.12.cloned.1.call-update
  8.9 2.4 collective-permute-start
  11.8 0.6 reduce-window.6
  12.4 0.2 slice_reduce_fusion
  13.2 1.4 scatter_custom_fusion
  14.8 0.6 fusion.39
  15.4 0.5 fusion.24
  16.1 0.3 copy.81
  16.4 0.2 fusion.49
  16.8 0.2 copy.85
  17.2 0.5 fusion.26
  17.7 0.9 multiply_reduce_fusion.4
  18.6 13.4 %all-gather.2 = f32[8,1,256]{2,1,0:T(1,128)S(1)} all-gather(f32[1,1,256]{2,1,0:T(1,128)S(1)} %bitcast.139), channel_id=3, replica_groups=mesh['sp'=8,'tp'=4] {'sp'}, dimensions={0}, use_global_device_ids=true | all-gather | bytes 9216 | tf_op jit(solution)/shard_map/all_gather | solution.py:13
  32.0 8.7 %all-gather = f32[2048,1]{0,1:T(1,128)S(1)} all-gather(f32[256,1]{0,1:T(1,128)S(1)} %get-tuple-element.288), channel_id=2, replica_groups=mesh['sp'=8,'tp'=4] {'sp'}, dimensions={0}, use_global_device_ids=true | all-gather | bytes 9216 | tf_op jit(solution)/shard_map/all_gather | solution.py:13
  40.7 0.6 broadcast.207
  41.3 0.7 reduce.5
  42.0 0.4 while.31
  42.5 126.3 %while.30 = (s32[]{:T(128)}, f32[256]{0:T(256)S(1)}, f32[256,512]{1,0:T(8,128)S(1)}, f32[256,512]{1,0:T(8,128)S(1)}, f32[256,512]{1,0:T(8,128)S(1)}, /*index=5*/...) while((s32[]{:T(128)}, f32[256]{0:T(256)S(1)}, f32[256,512]{1,0:T(8,128)S(1)}, ...), condition=%wide.region_7.8_spmd.clone, body=%wide.region_5.7_spmd.clone.sunk | while | flops 62963716 | bytes 2919583 | solution.py:84
  57.0 27.2 %fusion.83 = f32[256,1,128]{2,1,0:T(1,128)S(1)} fusion(f32[256,128,1]{1,2,0:T(1,128)S(1)} %bitcast.110, f32[256,128]{1,0:T(8,128)S(1)} %copy.123, pred[128,128]{1,0:T(8,128)(4,1)S(1)} %fusion.82), kind=kOutput, calls=%fused_computation.4.clone.1 | convolution fusion | flops 58720256 | bytes 409600 | tf_op jit(solution)/shard_map/while/body/eval_jaxpr/cts,cs->ct/dot_general | solution.py:71
  85.0 27.2 %fusion.83 = f32[256,1,128]{2,1,0:T(1,128)S(1)} fusion(f32[256,128,1]{1,2,0:T(1,128)S(1)} %bitcast.110, f32[256,128]{1,0:T(8,128)S(1)} %copy.123, pred[128,128]{1,0:T(8,128)(4,1)S(1)} %fusion.82), kind=kOutput, calls=%fused_computation.4.clone.1 | convolution fusion | flops 58720256 | bytes 409600 | tf_op jit(solution)/shard_map/while/body/eval_jaxpr/cts,cs->ct/dot_general | solution.py:71
  112.7 0.2 reduce_window_sum.57
  113.0 27.2 %fusion.83 = f32[256,1,128]{2,1,0:T(1,128)S(1)} fusion(f32[256,128,1]{1,2,0:T(1,128)S(1)} %bitcast.110, f32[256,128]{1,0:T(8,128)S(1)} %copy.123, pred[128,128]{1,0:T(8,128)(4,1)S(1)} %fusion.82), kind=kOutput, calls=%fused_computation.4.clone.1 | convolution fusion | flops 58720256 | bytes 409600 | tf_op jit(solution)/shard_map/while/body/eval_jaxpr/cts,cs->ct/dot_general | solution.py:71
  141.0 27.2 %fusion.83 = f32[256,1,128]{2,1,0:T(1,128)S(1)} fusion(f32[256,128,1]{1,2,0:T(1,128)S(1)} %bitcast.110, f32[256,128]{1,0:T(8,128)S(1)} %copy.123, pred[128,128]{1,0:T(8,128)(4,1)S(1)} %fusion.82), kind=kOutput, calls=%fused_computation.4.clone.1 | convolution fusion | flops 58720256 | bytes 409600 | tf_op jit(solution)/shard_map/while/body/eval_jaxpr/cts,cs->ct/dot_general | solution.py:71
  168.8 0.9 copy_bitcast_fusion.1
  169.7 3.7 %all-to-all-start = ((bf16[256,4,128]{2,0,1:T(8,128)(2,1)}), bf16[256,4,128]{2,0,1:T(8,128)(2,1)S(1)}, u32[]{:S(2)}, u32[]{:S(2)}) async-start(bf16[256,4,128]{2,0,1:T(8,128)(2,1)} %copy_bitcast_fusion.1), calls=%async_computation | async-start | bytes 524288 | tf_op jit(solution)/shard_map/all_to_all | solution.py:144
  173.4 5.9 %all-to-all-done = bf16[256,4,128]{2,0,1:T(8,128)(2,1)S(1)} async-done(((bf16[256,4,128]{2,0,1:T(8,128)(2,1)}), bf16[256,4,128]{2,0,1:T(8,128)(2,1)S(1)}, u32[]{:S(2)}, u32[]{:S(2)}) %all-to-all-start) | async-done | bytes 262176 | tf_op jit(solution)/shard_map/all_to_all | solution.py:144
  179.3 3.1 %multiply_reduce_fusion.3 = (f32[128]{0:T(128)S(1)}, f32[128,2048]{1,0:T(8,128)S(1)}) fusion(bf16[1024,128]{1,0:T(8,128)(2,1)S(1)} %bitcast.116, bf16[1024,2048]{1,0:T(8,128)(2,1)} %all-gather.8.cloned.1.call-done), kind=kOutput, calls=%fused_computation.46 | convolution fusion | flops 537395072 | bytes 5505536 | tf_op jit(solution)/shard_map/dot_general | solution.py:146
  182.4 0.4 multiply_reduce_fusion.2
  182.8 0.3 multiply_convert_fusion
  183.1 2.3 gather_fusion
  185.4 3.6 %all-to-all-start.1 = ((bf16[8,32,2048]{2,1,0:T(8,128)(2,1)}), bf16[8,32,2048]{2,1,0:T(8,128)(2,1)S(1)}, u32[]{:S(2)}, u32[]{:S(2)}) async-start(bf16[8,32,2048]{2,1,0:T(8,128)(2,1)} %bitcast.20), calls=%async_computation.1 | async-start | bytes 2097152 | tf_op jit(solution)/shard_map/all_to_all | solution.py:167
  189.0 26.5 %all-to-all-done.1 = bf16[8,32,2048]{2,1,0:T(8,128)(2,1)S(1)} async-done(((bf16[8,32,2048]{2,1,0:T(8,128)(2,1)}), bf16[8,32,2048]{2,1,0:T(8,128)(2,1)S(1)}, u32[]{:S(2)}, u32[]{:S(2)}) %all-to-all-start.1) | async-done | bytes 1048608 | tf_op jit(solution)/shard_map/all_to_all | solution.py:167
  215.5 2.3 fusion.16
  217.9 4.6 %fusion.12 = bf16[1,256,2048]{2,1,0:T(8,128)(2,1)} fusion(bf16[1,512,2048]{2,1,0:T(8,128)(2,1)} %all-gather.14.cloned.1.call-done, bf16[256,2048]{1,0:T(8,128)(2,1)S(1)} %bitcast.118, bf16[1,512,2048]{2,1,0:T(8,128)(2,1)} %all-gather.12.cloned.1.call-done, f32[256,512]{1,0:T(8,128)S(1)} %fusion.16), kind=kOutput, calls=%fused_computation.23 | convolution fusion | flops 1075052544 | bytes 6815744 | tf_op jit(solution)/shard_map/emk,ekd->emd/dot_general | solution.py:174
  222.5 2.8 copy.117
  225.3 0.5 broadcast.210
  225.8 7.8 %reduce.6 = bf16[256,2048]{1,0:T(8,128)(2,1)} reduce(bf16[256,1,2048]{2,1,0:T(2,128)(2,1)S(1)} %bitcast.109, bf16[]{:T(256)} %broadcast.210), dimensions={1}, to_apply=%bitcast.89.reduce_sub_computation | reduce | bytes 2097154
  233.6 2.6 reshape.255
  236.3 3.8 %all-to-all-start.2 = ((bf16[8,2,32768]{2,1,0:T(2,128)(2,1)}), bf16[8,2,32768]{2,1,0:T(2,128)(2,1)S(1)}, u32[]{:S(2)}, u32[]{:S(2)}) async-start(bf16[8,2,32768]{2,1,0:T(2,128)(2,1)} %reshape.255), calls=%async_computation.2 | async-start | bytes 2097152 | tf_op jit(solution)/shard_map/all_to_all | solution.py:175
  240.2 26.3 %all-to-all-done.2 = bf16[8,2,32768]{2,1,0:T(2,128)(2,1)S(1)} async-done(((bf16[8,2,32768]{2,1,0:T(2,128)(2,1)}), bf16[8,2,32768]{2,1,0:T(2,128)(2,1)S(1)}, u32[]{:S(2)}, u32[]{:S(2)}) %all-to-all-start.2) | async-done | bytes 1048608 | tf_op jit(solution)/shard_map/all_to_all | solution.py:175
  266.5 3.5 %reshape.256 = bf16[256,1,2048]{2,1,0:T(2,128)(2,1)} reshape(bf16[8,2,32768]{2,1,0:T(2,128)(2,1)S(1)} %all-to-all-done.2) | data formatting | bytes 2097152
  270.0 2.2 copy.115
  272.2 2.3 gather_fusion.1
  274.5 2.4 reshape.210
  276.9 3.2 %multiply_reduce_fusion = f32[128,2048]{1,0:T(8,128)S(1)} fusion(f32[128,2,2048]{2,1,0:T(2,128)S(1)} %reshape.210, f32[128,2]{1,0:T(8,128)S(1)} %copy.93), kind=kLoop, calls=%fused_computation.29 | loop fusion | flops 786432 | bytes 3146752 | tf_op jit(solution)/shard_map/reduce_sum | solution.py:180
  280.3 1.2 add_convert_fusion
  (130 shorter events, 5.1 us)
Async XLA Ops:
  6.5 8.9 %copy-start = (bf16[4,64,64]{2,1,0:T(8,128)(2,1)S(1)}, bf16[4,64,64]{2,1,0:T(8,128)(2,1)}, u32[]{:S(2)}) copy-start(bf16[4,64,64]{2,1,0:T(8,128)(2,1)} %param.25) | copy-start | bytes 98308
  6.5 2.3 copy-start.3
  6.5 4.8 %copy-start.10 = (s32[128,2]{0,1:T(2,128)S(1)}, s32[128,2]{0,1:T(2,128)}, u32[]{:S(2)}) copy-start(s32[128,2]{0,1:T(2,128)} %param.33) | copy-start | bytes 3076
  6.5 5.2 %copy-start.9 = (bf16[4,256]{1,0:T(4,128)(2,1)S(1)}, bf16[4,256]{1,0:T(4,128)(2,1)}, u32[]{:S(2)}) copy-start(bf16[4,256]{1,0:T(4,128)(2,1)} %param.24) | copy-start | bytes 6148
  6.5 5.3 %copy-start.12 = (f32[256]{0:T(256)S(1)}, f32[256]{0:T(256)}, u32[]{:S(2)}) copy-start(f32[256]{0:T(256)} %param.27) | copy-start | bytes 3076
  6.5 6.5 %copy-start.8 = (f32[512]{0:T(512)S(1)}, f32[512]{0:T(512)}, u32[]{:S(2)}) copy-start(f32[512]{0:T(512)} %param.28) | copy-start | bytes 6148
  6.6 172.7 %all-gather.8.cloned.1.call-start = ((), (), s32[]{:S(2)}) async-start(), calls=%async_computation.3 | async-start | bytes 5242880 | tf_op jit(solution)/shard_map/all_gather | solution.py:148
  7.3 181.7 %all-gather.10.cloned.1.call-start = ((), (), s32[]{:S(2)}) async-start(), calls=%async_computation.4 | async-start | bytes 2621440 | tf_op jit(solution)/shard_map/all_gather | solution.py:168
  8.0 209.8 %all-gather.12.cloned.1.call-start = ((), (), s32[]{:S(2)}) async-start(), calls=%async_computation.5 | async-start | bytes 2621440 | tf_op jit(solution)/shard_map/all_gather | solution.py:169
  8.8 209.1 %all-gather.14.cloned.1.call-start = ((), (), s32[]{:S(2)}) async-start(), calls=%async_computation.6 | async-start | bytes 2621440 | tf_op jit(solution)/shard_map/all_gather | solution.py:170
  8.9 5.7 %collective-permute-start = (bf16[256,3]{1,0:T(8,128)(2,1)S(1)}, bf16[256,3]{1,0:T(8,128)(2,1)S(1)}, u32[]{:S(2)}, u32[]{:S(2)}) collective-permute-start(bf16[256,3]{1,0:T(8,128)(2,1)S(1)} %slice.49), channel_id=1, source_target_pairs={{0,4},{4,8},{8,12},{12,16},{16,20},{20,24},{24,28},{1,5},{5,9},{9,... | collective-permute-start | bytes 4616 | tf_op jit(solution)/shard_map/ppermute | solution.py:31
  16.3 0.8 copy-start.13
  42.5 126.3 %copy-start.4 = (bf16[256,512]{1,0:T(8,128)(2,1)S(1)}, bf16[256,512]{1,0:T(8,128)(2,1)}, u32[]{:S(2)}) copy-start(bf16[256,512]{1,0:T(8,128)(2,1)} %param.23) | copy-start | bytes 786436
  169.7 9.6 %all-to-all-start = ((bf16[256,4,128]{2,0,1:T(8,128)(2,1)}), bf16[256,4,128]{2,0,1:T(8,128)(2,1)S(1)}, u32[]{:S(2)}, u32[]{:S(2)}) async-start(bf16[256,4,128]{2,0,1:T(8,128)(2,1)} %copy_bitcast_fusion.1), calls=%async_computation | async-start | bytes 524288 | tf_op jit(solution)/shard_map/all_to_all | solution.py:144
  179.3 3.1 %copy-start.1 = (bf16[128,2048]{1,0:T(8,128)(2,1)S(1)}, bf16[128,2048]{1,0:T(8,128)(2,1)}, u32[]{:S(2)}) copy-start(bf16[128,2048]{1,0:T(8,128)(2,1)} %param.21) | copy-start | bytes 1572868
  179.3 3.1 %copy-start.5 = (f32[2048]{0:T(1024)S(1)}, f32[2048]{0:T(1024)}, u32[]{:S(2)}) copy-start(f32[2048]{0:T(1024)} %param.30) | copy-start | bytes 24580
  179.3 3.5 %copy-start.6 = (f32[2048]{0:T(1024)S(1)}, f32[2048]{0:T(1024)}, u32[]{:S(2)}) copy-start(f32[2048]{0:T(1024)} %param.31) | copy-start | bytes 24580
  185.4 30.1 %all-to-all-start.1 = ((bf16[8,32,2048]{2,1,0:T(8,128)(2,1)}), bf16[8,32,2048]{2,1,0:T(8,128)(2,1)S(1)}, u32[]{:S(2)}, u32[]{:S(2)}) async-start(bf16[8,32,2048]{2,1,0:T(8,128)(2,1)} %bitcast.20), calls=%async_computation.1 | async-start | bytes 2097152 | tf_op jit(solution)/shard_map/all_to_all | solution.py:167
  233.6 6.4 %copy-start.11 = (f32[128,2]{0,1:T(2,128)S(1)}, f32[128,2]{0,1:T(2,128)}, u32[]{:S(2)}) copy-start(f32[128,2]{0,1:T(2,128)} %param.34) | copy-start | bytes 3076
  236.3 30.3 %all-to-all-start.2 = ((bf16[8,2,32768]{2,1,0:T(2,128)(2,1)}), bf16[8,2,32768]{2,1,0:T(2,128)(2,1)S(1)}, u32[]{:S(2)}, u32[]{:S(2)}) async-start(bf16[8,2,32768]{2,1,0:T(2,128)(2,1)} %reshape.255), calls=%async_computation.2 | async-start | bytes 2097152 | tf_op jit(solution)/shard_map/all_to_all | solution.py:175
  276.9 3.4 %copy-start.2 = (bf16[128,2048]{1,0:T(8,128)(2,1)S(1)}, bf16[128,2048]{1,0:T(8,128)(2,1)}, u32[]{:S(2)}) copy-start(bf16[128,2048]{1,0:T(8,128)(2,1)} %param.21) | copy-start | bytes 1572868
  276.9 3.4 %copy-start.7 = (f32[2048]{0:T(1024)S(1)}, f32[2048]{0:T(1024)}, u32[]{:S(2)}) copy-start(f32[2048]{0:T(1024)} %param.32) | copy-start | bytes 24580
Sparse Core Ops, SparseCore 0:
  9.2 55.2 all-gather.7
  66.4 35.1 all-gather.9
  103.4 35.1 all-gather.11
  140.4 35.1 all-gather.13
where the time goes:
time: 293 us; the launch traced here: 288 us
  matrix products  120 us (41%)
  waiting for transfers between devices  60.8 us (21%)
  local copies, waits for them, and re-layouts  24.8 us (8%)
  blocking collectives  22.1 us (8%)
  other arithmetic  18.4 us (6%)
  loops' own time  14.9 us (5%)
  between operations  13.8 us (5%)
  starting transfers between devices  13.6 us (5%)
    dot_general x4, matrix products, one_block(): jnp.einsum('cts,cs->ct', jnp.exp(gap), block_drive, precision=lax.Precisi...  109 us
    all_to_all x1, waiting for transfers between devices, per_device(): lax.all_to_all(outgoing, 'sp', split_axis=0, concat_axis=1, tiled=True)  26.5 us
    all_to_all x1, waiting for transfers between devices, per_device(): lax.all_to_all(result.astype(jnp.bfloat16), 'sp', split_axis=1, concat_ax...  26.3 us
    all_gather x2, blocking collectives, entering_2(): everything = jax.tree.map(lambda part: lax.all_gather(part, axis), array)  22.1 us
    another operation x1, loops' own time, block_recurrence(): _, _, hidden_state, summed_log = lax.fori_loop(0, count, one_block, initial)  14.7 us
    unnamed x36, local copies, waits for them, and re-layouts  9.28 us
    unnamed x2, other arithmetic  7.79 us
  transfers between devices with their start and end apart: 8, of which 3 were waited for; matrix products, arithmetic and copies ran while one was open for 45% of the time, Pallas kernels for 0%

commit v1 on v0

--- a/solution.py
+++ b/solution.py
@@ -172,8 +172,14 @@
     up_vals = jnp.einsum("emd,ekd->emk", arriving, up_rows, preferred_element_type=jnp.float32)
     hidden = (jax.nn.silu(gate_vals) * up_vals).astype(jnp.bfloat16)
     result = jnp.einsum("emk,ekd->emd", hidden, down_rows, preferred_element_type=jnp.float32)
-    returned = lax.all_to_all(
-        result.astype(jnp.bfloat16), "sp", split_axis=1, concat_axis=0, tiled=True
+    returned = jnp.concatenate(
+        lax.all_to_all(
+            jnp.stack(jnp.split(result.astype(jnp.bfloat16), lax.axis_size("sp"), axis=1)),
+            "sp",
+            0,
+            0,
+        ),
+        axis=0,
     )
     returned = returned.reshape(experts * capacity, returned.shape[2])
     picked = returned[target].astype(jnp.float32).reshape(token_count, top_count, returned.shape[1])

time: 293 us -> 279 us (0.952)
  other arithmetic: 18.4 us -> 10.7 us
  local copies, waits for them, and re-layouts: 24.8 us -> 18.4 us
    unnamed x2 -> x1, other arithmetic: 7.79 us -> 0.01 us
    unnamed x36 -> x39, local copies, waits for them, and re-layouts: 9.28 us -> 5.11 us
  transfers between devices with their start and end apart: 8 -> 8, of which waited for: 3 -> 3; matrix products, arithmetic and copies ran while one was open for 45% -> 48% of each run, Pallas kernels for 0% -> 0%
where the time goes in v1:
time: 279 us; the launch traced here: 274 us
  matrix products  120 us (43%)
  waiting for transfers between devices  60.8 us (22%)
  blocking collectives  22.1 us (8%)
  local copies, waits for them, and re-layouts  18.4 us (7%)
  loops' own time  14.8 us (5%)
  between operations  13.9 us (5%)
  starting transfers between devices  13.4 us (5%)
  other arithmetic  10.7 us (4%)
    dot_general x4, matrix products, one_block(): jnp.einsum('cts,cs->ct', jnp.exp(gap), block_drive, precision=lax.Precisi...  109 us
    all_to_all x1, waiting for transfers between devices, per_device(): lax.all_to_all(outgoing, 'sp', split_axis=0, concat_axis=1, tiled=True)  26.5 us
    all_to_all x1, waiting for transfers between devices, per_device(): lax.all_to_all(jnp.stack(jnp.split(result.astype(jnp.bfloat16), lax.axis_...  26.4 us
    all_gather x2, blocking collectives, entering_2(): everything = jax.tree.map(lambda part: lax.all_gather(part, axis), array)  22.1 us
    another operation x1, loops' own time, block_recurrence(): _, _, hidden_state, summed_log = lax.fori_loop(0, count, one_block, initial)  14.6 us
    all_to_all x1, waiting for transfers between devices, per_device(): lax.all_to_all(branch_out, 'tp', split_axis=1, concat_axis=0, tiled=True)  5.86 us
  transfers between devices with their start and end apart: 8, of which 3 were waited for; matrix products, arithmetic and copies ran while one was open for 48% of the time, Pallas kernels for 0%

profile of v1, /device:TPU:0, one launch (start us, length us, event | category | flops | bytes accessed | tf_op | source)
XLA Modules:
  0.0 274.0 jit_solution(13760332130114189561)
XLA Ops:
  6.6 0.7 all-gather.8.cloned.1.call-update
  7.3 0.7 all-gather.10.cloned.1.call-update
  8.1 0.7 all-gather.12.cloned.1.call-update
  8.9 2.4 collective-permute-start
  11.8 0.6 reduce-window.6
  12.4 0.2 slice_reduce_fusion
  13.2 1.4 scatter_custom_fusion
  14.8 0.6 fusion.39
  15.4 0.5 fusion.24
  16.1 0.3 copy.65
  16.4 0.2 fusion.49
  17.2 0.5 fusion.26
  17.7 0.9 multiply_reduce_fusion.4
  18.6 13.4 %all-gather.2 = f32[8,1,256]{2,1,0:T(1,128)S(1)} all-gather(f32[1,1,256]{2,1,0:T(1,128)S(1)} %bitcast.163), channel_id=3, replica_groups=mesh['sp'=8,'tp'=4] {'sp'}, dimensions={0}, use_global_device_ids=true | all-gather | bytes 9216 | tf_op jit(solution)/shard_map/all_gather | solution.py:13
  32.0 8.7 %all-gather = f32[2048,1]{0,1:T(1,128)S(1)} all-gather(f32[256,1]{0,1:T(1,128)S(1)} %get-tuple-element.283), channel_id=2, replica_groups=mesh['sp'=8,'tp'=4] {'sp'}, dimensions={0}, use_global_device_ids=true | all-gather | bytes 9216 | tf_op jit(solution)/shard_map/all_gather | solution.py:13
  40.8 0.5 broadcast.207
  41.3 0.6 reduce.5
  41.9 0.4 while.31
  42.5 126.2 %while.30 = (s32[]{:T(128)}, f32[256]{0:T(256)S(1)}, f32[256,512]{1,0:T(8,128)S(1)}, f32[256,512]{1,0:T(8,128)S(1)}, f32[256,512]{1,0:T(8,128)S(1)}, /*index=5*/...) while((s32[]{:T(128)}, f32[256]{0:T(256)S(1)}, f32[256,512]{1,0:T(8,128)S(1)}, ...), condition=%wide.region_7.8_spmd.clone, body=%wide.region_5.7_spmd.clone.sunk | while | flops 62963716 | bytes 2919583 | solution.py:84
  56.9 27.2 %fusion.91 = f32[256,1,128]{2,1,0:T(1,128)S(1)} fusion(f32[256,128,1]{1,2,0:T(1,128)S(1)} %bitcast.134, f32[256,128]{1,0:T(8,128)S(1)} %copy.101, pred[128,128]{1,0:T(8,128)(4,1)S(1)} %fusion.90), kind=kOutput, calls=%fused_computation.4.clone.1 | convolution fusion | flops 58720256 | bytes 409600 | tf_op jit(solution)/shard_map/while/body/eval_jaxpr/cts,cs->ct/dot_general | solution.py:71
  84.9 27.2 %fusion.91 = f32[256,1,128]{2,1,0:T(1,128)S(1)} fusion(f32[256,128,1]{1,2,0:T(1,128)S(1)} %bitcast.134, f32[256,128]{1,0:T(8,128)S(1)} %copy.101, pred[128,128]{1,0:T(8,128)(4,1)S(1)} %fusion.90), kind=kOutput, calls=%fused_computation.4.clone.1 | convolution fusion | flops 58720256 | bytes 409600 | tf_op jit(solution)/shard_map/while/body/eval_jaxpr/cts,cs->ct/dot_general | solution.py:71
  112.9 27.2 %fusion.91 = f32[256,1,128]{2,1,0:T(1,128)S(1)} fusion(f32[256,128,1]{1,2,0:T(1,128)S(1)} %bitcast.134, f32[256,128]{1,0:T(8,128)S(1)} %copy.101, pred[128,128]{1,0:T(8,128)(4,1)S(1)} %fusion.90), kind=kOutput, calls=%fused_computation.4.clone.1 | convolution fusion | flops 58720256 | bytes 409600 | tf_op jit(solution)/shard_map/while/body/eval_jaxpr/cts,cs->ct/dot_general | solution.py:71
  140.9 27.2 %fusion.91 = f32[256,1,128]{2,1,0:T(1,128)S(1)} fusion(f32[256,128,1]{1,2,0:T(1,128)S(1)} %bitcast.134, f32[256,128]{1,0:T(8,128)S(1)} %copy.101, pred[128,128]{1,0:T(8,128)(4,1)S(1)} %fusion.90), kind=kOutput, calls=%fused_computation.4.clone.1 | convolution fusion | flops 58720256 | bytes 409600 | tf_op jit(solution)/shard_map/while/body/eval_jaxpr/cts,cs->ct/dot_general | solution.py:71
  168.6 0.9 copy_bitcast_fusion
  169.5 3.7 %all-to-all-start = ((bf16[256,4,128]{2,0,1:T(8,128)(2,1)}), bf16[256,4,128]{2,0,1:T(8,128)(2,1)S(1)}, u32[]{:S(2)}, u32[]{:S(2)}) async-start(bf16[256,4,128]{2,0,1:T(8,128)(2,1)} %copy_bitcast_fusion), calls=%async_computation | async-start | bytes 524288 | tf_op jit(solution)/shard_map/all_to_all | solution.py:144
  173.3 5.9 %all-to-all-done = bf16[256,4,128]{2,0,1:T(8,128)(2,1)S(1)} async-done(((bf16[256,4,128]{2,0,1:T(8,128)(2,1)}), bf16[256,4,128]{2,0,1:T(8,128)(2,1)S(1)}, u32[]{:S(2)}, u32[]{:S(2)}) %all-to-all-start) | async-done | bytes 262176 | tf_op jit(solution)/shard_map/all_to_all | solution.py:144
  179.1 3.1 %multiply_reduce_fusion.3 = (f32[128]{0:T(128)S(1)}, f32[128,2048]{1,0:T(8,128)S(1)}) fusion(bf16[1024,128]{1,0:T(8,128)(2,1)S(1)} %bitcast.140, bf16[1024,2048]{1,0:T(8,128)(2,1)} %all-gather.8.cloned.1.call-done), kind=kOutput, calls=%fused_computation.45 | convolution fusion | flops 537395072 | bytes 5505536 | tf_op jit(solution)/shard_map/dot_general | solution.py:146
  182.2 0.4 multiply_reduce_fusion.2
  182.6 0.3 multiply_convert_fusion
  182.9 2.3 gather_fusion
  185.3 3.6 %all-to-all-start.1 = ((bf16[8,32,2048]{2,1,0:T(8,128)(2,1)}), bf16[8,32,2048]{2,1,0:T(8,128)(2,1)S(1)}, u32[]{:S(2)}, u32[]{:S(2)}) async-start(bf16[8,32,2048]{2,1,0:T(8,128)(2,1)} %bitcast.20), calls=%async_computation.1 | async-start | bytes 2097152 | tf_op jit(solution)/shard_map/all_to_all | solution.py:167
  188.9 26.5 %all-to-all-done.1 = bf16[8,32,2048]{2,1,0:T(8,128)(2,1)S(1)} async-done(((bf16[8,32,2048]{2,1,0:T(8,128)(2,1)}), bf16[8,32,2048]{2,1,0:T(8,128)(2,1)S(1)}, u32[]{:S(2)}, u32[]{:S(2)}) %all-to-all-start.1) | async-done | bytes 1048608 | tf_op jit(solution)/shard_map/all_to_all | solution.py:167
  215.4 3.1 %fusion.16 = f32[256,512]{1,0:T(8,128)} fusion(bf16[256,2048]{1,0:T(8,128)(2,1)S(1)} %bitcast.141, bf16[1,512,2048]{2,1,0:T(8,128)(2,1)} %all-gather.10.cloned.1.call-done), kind=kOutput, calls=%fused_computation.27 | convolution fusion | flops 536870912 | bytes 3670016 | tf_op jit(solution)/shard_map/emd,ekd->emk/dot_general | solution.py:171
  218.5 3.8 %fusion.12 = bf16[1,256,2048]{2,1,0:T(8,128)(2,1)S(1)} fusion(bf16[1,512,2048]{2,1,0:T(8,128)(2,1)} %all-gather.14.cloned.1.call-done, bf16[256,2048]{1,0:T(8,128)(2,1)S(1)} %bitcast.142, bf16[1,512,2048]{2,1,0:T(8,128)(2,1)} %all-gather.12.cloned.1.call-done, f32[256,512]{1,0:T(8,128)} %fusion.16), kind=kOutput, calls=%fused_computation.23 | convolution fusion | flops 1075052544 | bytes 6815744 | tf_op jit(solution)/shard_map/emk,ekd->emd/dot_general | solution.py:174
  222.4 0.7 fusion.63
  223.0 0.7 fusion.62
  223.7 0.7 fusion.61
  224.3 0.6 fusion.60
  225.0 0.7 fusion.59
  225.7 0.7 fusion.58
  226.3 0.7 fusion.57
  227.0 0.7 fusion.56
  227.7 3.6 %all-to-all-start.2 = ((bf16[8,1,32,2048]{3,2,1,0:T(8,128)(2,1)}), bf16[8,1,32,2048]{3,2,1,0:T(8,128)(2,1)S(1)}, u32[]{:S(2)}, u32[]{:S(2)}) async-start(bf16[8,1,32,2048]{3,2,1,0:T(8,128)(2,1)} %fusion.56), calls=%async_computation.2 | async-start | bytes 2097152 | tf_op jit(solution)/shard_map/all_to_all | solution.py:176
  231.3 26.4 %all-to-all-done.2 = bf16[8,1,32,2048]{3,2,1,0:T(8,128)(2,1)S(1)} async-done(((bf16[8,1,32,2048]{3,2,1,0:T(8,128)(2,1)}), bf16[8,1,32,2048]{3,2,1,0:T(8,128)(2,1)S(1)}, u32[]{:S(2)}, u32[]{:S(2)}) %all-to-all-start.2) | async-done | bytes 1048608 | tf_op jit(solution)/shard_map/all_to_all | solution.py:176
  257.7 2.3 gather_fusion.1
  260.0 2.4 reshape.202
  262.4 3.3 %multiply_reduce_fusion = f32[128,2048]{1,0:T(8,128)S(1)} fusion(f32[128,2,2048]{2,1,0:T(2,128)S(1)} %reshape.202, f32[128,2]{1,0:T(8,128)S(1)} %copy.76), kind=kLoop, calls=%fused_computation.29 | loop fusion | flops 786432 | bytes 3146752 | tf_op jit(solution)/shard_map/reduce_sum | solution.py:186
  265.9 1.2 add_convert_fusion
  (132 shorter events, 5.5 us)
Async XLA Ops:
  6.5 8.9 %copy-start = (bf16[4,64,64]{2,1,0:T(8,128)(2,1)S(1)}, bf16[4,64,64]{2,1,0:T(8,128)(2,1)}, u32[]{:S(2)}) copy-start(bf16[4,64,64]{2,1,0:T(8,128)(2,1)} %param.25) | copy-start | bytes 98308
  6.5 2.3 copy-start.3
  6.5 4.8 %copy-start.10 = (s32[128,2]{0,1:T(2,128)S(1)}, s32[128,2]{0,1:T(2,128)}, u32[]{:S(2)}) copy-start(s32[128,2]{0,1:T(2,128)} %param.33) | copy-start | bytes 3076
  6.5 5.2 %copy-start.9 = (bf16[4,256]{1,0:T(4,128)(2,1)S(1)}, bf16[4,256]{1,0:T(4,128)(2,1)}, u32[]{:S(2)}) copy-start(bf16[4,256]{1,0:T(4,128)(2,1)} %param.24) | copy-start | bytes 6148
  6.5 5.3 %copy-start.12 = (f32[256]{0:T(256)S(1)}, f32[256]{0:T(256)}, u32[]{:S(2)}) copy-start(f32[256]{0:T(256)} %param.27) | copy-start | bytes 3076
  6.5 6.5 %copy-start.8 = (f32[512]{0:T(512)S(1)}, f32[512]{0:T(512)}, u32[]{:S(2)}) copy-start(f32[512]{0:T(512)} %param.28) | copy-start | bytes 6148
  6.6 172.6 %all-gather.8.cloned.1.call-start = ((), (), s32[]{:S(2)}) async-start(), calls=%async_computation.3 | async-start | bytes 5242880 | tf_op jit(solution)/shard_map/all_gather | solution.py:148
  7.3 181.6 %all-gather.10.cloned.1.call-start = ((), (), s32[]{:S(2)}) async-start(), calls=%async_computation.4 | async-start | bytes 2621440 | tf_op jit(solution)/shard_map/all_gather | solution.py:168
  8.0 210.5 %all-gather.12.cloned.1.call-start = ((), (), s32[]{:S(2)}) async-start(), calls=%async_computation.5 | async-start | bytes 2621440 | tf_op jit(solution)/shard_map/all_gather | solution.py:169
  8.8 209.8 %all-gather.14.cloned.1.call-start = ((), (), s32[]{:S(2)}) async-start(), calls=%async_computation.6 | async-start | bytes 2621440 | tf_op jit(solution)/shard_map/all_gather | solution.py:170
  8.9 5.7 %collective-permute-start = (bf16[256,3]{1,0:T(8,128)(2,1)S(1)}, bf16[256,3]{1,0:T(8,128)(2,1)S(1)}, u32[]{:S(2)}, u32[]{:S(2)}) collective-permute-start(bf16[256,3]{1,0:T(8,128)(2,1)S(1)} %slice.49), channel_id=1, source_target_pairs={{0,4},{4,8},{8,12},{12,16},{16,20},{20,24},{24,28},{1,5},{5,9},{9,... | collective-permute-start | bytes 4616 | tf_op jit(solution)/shard_map/ppermute | solution.py:31
  16.4 0.8 copy-start.13
  42.4 126.2 %copy-start.4 = (bf16[256,512]{1,0:T(8,128)(2,1)S(1)}, bf16[256,512]{1,0:T(8,128)(2,1)}, u32[]{:S(2)}) copy-start(bf16[256,512]{1,0:T(8,128)(2,1)} %param.23) | copy-start | bytes 786436
  169.5 9.6 %all-to-all-start = ((bf16[256,4,128]{2,0,1:T(8,128)(2,1)}), bf16[256,4,128]{2,0,1:T(8,128)(2,1)S(1)}, u32[]{:S(2)}, u32[]{:S(2)}) async-start(bf16[256,4,128]{2,0,1:T(8,128)(2,1)} %copy_bitcast_fusion), calls=%async_computation | async-start | bytes 524288 | tf_op jit(solution)/shard_map/all_to_all | solution.py:144
  179.1 3.1 %copy-start.1 = (bf16[128,2048]{1,0:T(8,128)(2,1)S(1)}, bf16[128,2048]{1,0:T(8,128)(2,1)}, u32[]{:S(2)}) copy-start(bf16[128,2048]{1,0:T(8,128)(2,1)} %param.21) | copy-start | bytes 1572868
  179.1 3.1 %copy-start.5 = (f32[2048]{0:T(1024)S(1)}, f32[2048]{0:T(1024)}, u32[]{:S(2)}) copy-start(f32[2048]{0:T(1024)} %param.30) | copy-start | bytes 24580
  179.1 3.5 %copy-start.6 = (f32[2048]{0:T(1024)S(1)}, f32[2048]{0:T(1024)}, u32[]{:S(2)}) copy-start(f32[2048]{0:T(1024)} %param.31) | copy-start | bytes 24580
  185.3 30.1 %all-to-all-start.1 = ((bf16[8,32,2048]{2,1,0:T(8,128)(2,1)}), bf16[8,32,2048]{2,1,0:T(8,128)(2,1)S(1)}, u32[]{:S(2)}, u32[]{:S(2)}) async-start(bf16[8,32,2048]{2,1,0:T(8,128)(2,1)} %bitcast.20), calls=%async_computation.1 | async-start | bytes 2097152 | tf_op jit(solution)/shard_map/all_to_all | solution.py:167
  222.3 8.9 %copy-start.11 = (f32[128,2]{0,1:T(2,128)S(1)}, f32[128,2]{0,1:T(2,128)}, u32[]{:S(2)}) copy-start(f32[128,2]{0,1:T(2,128)} %param.34) | copy-start | bytes 3076
  227.7 30.1 %all-to-all-start.2 = ((bf16[8,1,32,2048]{3,2,1,0:T(8,128)(2,1)}), bf16[8,1,32,2048]{3,2,1,0:T(8,128)(2,1)S(1)}, u32[]{:S(2)}, u32[]{:S(2)}) async-start(bf16[8,1,32,2048]{3,2,1,0:T(8,128)(2,1)} %fusion.56), calls=%async_computation.2 | async-start | bytes 2097152 | tf_op jit(solution)/shard_map/all_to_all | solution.py:176
  262.4 3.5 %copy-start.2 = (bf16[128,2048]{1,0:T(8,128)(2,1)S(1)}, bf16[128,2048]{1,0:T(8,128)(2,1)}, u32[]{:S(2)}) copy-start(bf16[128,2048]{1,0:T(8,128)(2,1)} %param.21) | copy-start | bytes 1572868
  262.4 3.5 %copy-start.7 = (f32[2048]{0:T(1024)S(1)}, f32[2048]{0:T(1024)}, u32[]{:S(2)}) copy-start(f32[2048]{0:T(1024)} %param.32) | copy-start | bytes 24580
Sparse Core Ops, SparseCore 0:
  9.2 55.2 all-gather.7
  66.4 35.1 all-gather.9
  103.4 35.1 all-gather.11
  140.4 35.1 all-gather.13
